TPU v7x, 256 devices: a 4x2x16 block of a 4x16x16 slice. The times are simulated.
256 devices in a mesh: grp: 2 (over y), ep: 32 (over z, core), tp: 4 (over x).
Axes of the slice: x: 4, y: 2, z: 16, core: 2. Of those that a mesh axis runs over, the one named last changes fastest.
The devices are a block of a 4x16x16 slice.
Arguments:
- x_in: bfloat16 [4096, 2048], P(('grp', 'ep')), parts along dimension 0, may hold values from -6 to 6
- state: float32 [4096, 96, 128], P(('grp', 'ep'), 'tp'), parts along dimension 0, may hold values from -6 to 6
- routes: int32 [4096, 2], P(('grp', 'ep')), parts along dimension 0, may hold values from 0 to 63, as said below
- w_in: bfloat16 [2048, 1536], P(None, 'tp'), may hold values from -0.125 to 0.125
- decay_rate: float32 [96, 64], P('tp'), may hold values from 0.01 to 1
- frequency: float32 [96, 64], P('tp'), may hold values from 0 to 192
- log_step: float32 [96], P('tp'), may hold values from -3 to 0
- b_in: float32 [96, 16, 128], P('tp'), may hold values from -1.5 to 1.5
- c_out: float32 [96, 16, 128], P('tp'), may hold values from -0.5 to 0.5
- skip: float32 [1536], P('tp'), may hold values from -3 to 3
- w_out: bfloat16 [1536, 2048], P('tp'), may hold values from -0.15625 to 0.15625
- gain_mix: float32 [2048], replicated, may hold values from 0.1 to 1.9
- w_group: bfloat16 [2048, 4], replicated, may hold values from -0.0625 to 0.0625
- w_expert: bfloat16 [2048, 64], replicated, may hold values from -0.0625 to 0.0625
- w_gate: bfloat16 [64, 2048, 1024], P('ep', None, 'tp'), may hold values from -0.125 to 0.125
- w_up: bfloat16 [64, 2048, 1024], P('ep', None, 'tp'), may hold values from -0.125 to 0.125
- w_down: bfloat16 [64, 1024, 2048], P('ep', 'tp'), may hold values from -3 to 3
- gain_moe: float32 [2048], replicated, may hold values from 0.1 to 1.9
Outputs:
- layer_out: bfloat16 [4096, 2048], P(('grp', 'ep')), parts along dimension 0
- new_state: float32 [4096, 96, 128], P(('grp', 'ep'), 'tp'), parts along dimension 0
There are 2 independent parts, one for each index of `grp`. A program takes and returns all parts, laid end to end along the dimension named above; an argument that names none is the same for every part. Nothing has to cross between parts.
Inputs may be any that keep to these rules, and one draw needn't show every extreme that they name: `routes`: each row names two different experts of one group of 16 consecutive expert numbers. Within the rows of one index of ep (aligned blocks of 64 rows) no expert is named by more than 4 rows, and in every block some expert is named by exactly 4 rows.
All inputs are finite; a program needn't handle non-finite values.
Results may differ from a plain program's by a relative error of at most 0.015.
Values may be sent and summed in bfloat16 or wider, within the bound.
A program may use at most 64 MiB of HBM per device.

v0:
```python
import jax
import jax.numpy as jnp
from jax import lax
from jax.sharding import PartitionSpec as P

residual_scale = 8.0**0.25
norm_eps = 1e-05


def sent_to_all(x, axis):
    devices = lax.axis_size(axis)
    return lax.all_to_all(jnp.broadcast_to(x[None], (devices, *x.shape)), axis, 0, 0, tiled=True)


def taken_together(x, axis):
    everything = sent_to_all(x, axis)
    return jnp.sum(everything.astype(jnp.float32), axis=0)


def in_order(parts, dim):
    lengths = list(parts.shape[1:])
    lengths[dim] *= parts.shape[0]
    return jnp.moveaxis(parts, 0, dim).reshape(lengths)


def gather_directly(x, axis, dim):
    parts = sent_to_all(x, axis)
    return in_order(parts, dim)


def split_up(x, dim, devices):
    before, after = (x.shape[:dim], x.shape[dim + 1 :])
    return jnp.moveaxis(x.reshape(*before, devices, -1, *after), dim, 0)


def sent_and_summed(x, axis, dim):
    devices = lax.axis_size(axis)
    parts = lax.all_to_all(split_up(x, dim, devices), axis, 0, 0, tiled=True)
    return jnp.sum(parts.astype(jnp.float32), axis=0)


def normalize(values, gain):
    centre = jnp.mean(values, -1, keepdims=True)
    spread = jnp.mean(jnp.square(values - centre), -1, keepdims=True)
    return (values - centre) * lax.rsqrt(spread + norm_eps) * gain


def s5_advance(mix_input, state, decay_rate, frequency, log_step, b_in, c_out, skip):
    top_precision = lax.Precision.DEFAULT
    entries = decay_rate.shape[-1]
    group_count = decay_rate.shape[0]
    width = b_in.shape[1]
    seq_count = mix_input.shape[0]
    input_rows = mix_input.astype(jnp.float32).reshape(seq_count, group_count, width)
    step_size = jnp.exp(log_step)[:, None]
    lam_real = -decay_rate
    magnitude = jnp.exp(lam_real * step_size)
    angle_dt = frequency * step_size
    bar_real = magnitude * jnp.cos(angle_dt)
    bar_imag = magnitude * jnp.sin(angle_dt)
    minus_real = bar_real - 1.0
    modulus = lam_real * lam_real + frequency * frequency
    ratio_real = (minus_real * lam_real + bar_imag * frequency) / modulus
    ratio_imag = (bar_imag * lam_real - minus_real * frequency) / modulus
    in_real = b_in[..., :entries]
    in_imag = b_in[..., entries:]
    input_matrix_real = ratio_real[:, None, :] * in_real - ratio_imag[:, None, :] * in_imag
    input_matrix_imag = ratio_real[:, None, :] * in_imag + ratio_imag[:, None, :] * in_real
    forcing_real = jnp.einsum(
        "rxf,xfb->rxb", input_rows, input_matrix_real, precision=top_precision
    )
    forcing_imag = jnp.einsum(
        "rxf,xfb->rxb", input_rows, input_matrix_imag, precision=top_precision
    )
    old_real = state[..., :entries]
    old_imag = state[..., entries:]
    following_real = bar_real * old_real - bar_imag * old_imag + forcing_real
    following_imag = bar_real * old_imag + bar_imag * old_real + forcing_imag
    output_real = c_out[..., :entries]
    output_imag = c_out[..., entries:]
    output_matrix = jnp.einsum("lzt,zft->lzf", following_real, output_real, precision=top_precision)
    output_matrix = output_matrix - jnp.einsum(
        "lzt,zft->lzf", following_imag, output_imag, precision=top_precision
    )
    output_matrix = output_matrix + skip.reshape(group_count, width) * input_rows
    activated = jax.nn.gelu(output_matrix).reshape(seq_count, group_count * width)
    return (activated, jnp.concatenate([following_real, following_imag], axis=-1))


def route_weights(normed, routes, w_group, w_expert):
    group_total = w_group.shape[1]
    expert_total = w_expert.shape[1]
    per_group = expert_total // group_total
    group_logit = jnp.dot(normed, w_group, preferred_element_type=jnp.float32)
    group_exp = jnp.exp(group_logit)
    group_prob = group_exp / jnp.sum(group_exp, -1, keepdims=True)
    chosen = routes[:, 0] // per_group
    group_pick = jnp.sum(
        jnp.where(
            chosen[:, None] == jnp.arange(group_total, dtype=jnp.int32)[None, :], group_prob, 0.0
        ),
        -1,
    )
    expert_logit = jnp.dot(normed, w_expert, preferred_element_type=jnp.float32)
    picked = jnp.sum(
        jnp.where(
            routes[:, :, None] == jnp.arange(expert_total, dtype=jnp.int32)[None, None, :],
            expert_logit[:, None, :],
            0.0,
        ),
        -1,
    )
    pair_exp = jnp.exp(picked)
    return pair_exp / jnp.sum(pair_exp, -1, keepdims=True) * group_pick[:, None]


def per_device(
    x_in,
    state,
    routes,
    w_in,
    decay_rate,
    frequency,
    log_step,
    b_in,
    c_out,
    skip,
    w_out,
    gain_mix,
    w_group,
    w_expert,
    w_gate,
    w_up,
    w_down,
    gain_moe,
):
    top_precision = lax.Precision.DEFAULT
    seq_count = x_in.shape[0]
    model_width = x_in.shape[1]
    mix_input = jnp.dot(x_in, w_in, preferred_element_type=jnp.float32).astype(jnp.bfloat16)
    activated, new_state = s5_advance(
        mix_input, state, decay_rate, frequency, log_step, b_in, c_out, skip
    )
    partial_mix = jnp.dot(activated.astype(jnp.bfloat16), w_out, preferred_element_type=jnp.float32)
    mixed = taken_together(partial_mix.astype(jnp.bfloat16), "tp").astype(jnp.float32)
    hidden_state = normalize(residual_scale * x_in.astype(jnp.float32) + mixed, gain_mix)
    hidden_bf = hidden_state.astype(jnp.bfloat16)
    route_weight = route_weights(hidden_bf, routes, w_group, w_expert)
    expert_total = w_expert.shape[1]
    ep_count = lax.axis_size("ep")
    local_experts = w_gate.shape[0]
    capacity = max(2, 4 * seq_count // expert_total)
    total_slots = expert_total * capacity
    hits = (routes[:, :, None] == jnp.arange(expert_total, dtype=jnp.int32)[None, None, :]).astype(
        jnp.int32
    )
    tally = jnp.sum(hits, axis=1)
    prior = jnp.cumsum(tally, axis=0) - tally
    slot_in_block = jnp.sum(prior[:, None, :] * hits, axis=-1)
    target = routes * capacity + slot_in_block
    slot_ids = jnp.arange(total_slots, dtype=jnp.int32)
    matches = target[:, :, None] == slot_ids[None, None, :]
    dispatch_map = jnp.any(slot_ids[:, None, None] == target[None, :, :], axis=-1).astype(
        jnp.bfloat16
    )
    combine_map = jnp.sum(jnp.where(matches, route_weight[:, :, None], 0.0), axis=1)
    buffer = jnp.dot(dispatch_map, hidden_bf, preferred_element_type=jnp.float32).astype(
        jnp.bfloat16
    )
    buffer = buffer.reshape(ep_count, local_experts, capacity, model_width)
    column_width = model_width // lax.axis_size("tp")
    own_columns = lax.dynamic_slice_in_dim(
        buffer, lax.axis_index("tp") * column_width, column_width, 3
    )
    piece = gather_directly(
        lax.all_to_all(own_columns, "ep", split_axis=0, concat_axis=0, tiled=True), "tp", 3
    )
    gate_part = jnp.einsum("njcd,jdf->njcf", piece, w_gate, preferred_element_type=jnp.float32)
    up_part = jnp.einsum("njcd,jdf->njcf", piece, w_up, preferred_element_type=jnp.float32)
    act = (jax.nn.silu(gate_part) * up_part).astype(jnp.bfloat16)
    share = sent_and_summed(
        jnp.einsum("njcf,jfd->njcd", act, w_down, preferred_element_type=jnp.float32).astype(
            jnp.bfloat16
        ),
        "tp",
        3,
    ).astype(jnp.bfloat16)
    returned_rows = lax.all_to_all(share, "ep", split_axis=0, concat_axis=0, tiled=True)
    flat_rows = returned_rows.reshape(total_slots, returned_rows.shape[3])
    moe = jnp.dot(
        combine_map,
        lax.all_gather(flat_rows, "tp", axis=1, tiled=True).astype(jnp.float32),
        precision=top_precision,
    )
    layer_out = normalize(residual_scale * hidden_state + moe, gain_moe).astype(jnp.bfloat16)
    return (layer_out, new_state)


def solution(mesh):
    in_specs = (
        P(("grp", "ep"), None),
        P(("grp", "ep"), "tp", None),
        P(("grp", "ep"), None),
        P(None, "tp"),
        P("tp", None),
        P("tp", None),
        P("tp"),
        P("tp", None, None),
        P("tp", None, None),
        P("tp"),
        P("tp", None),
        P(),
        P(),
        P(),
        P("ep", None, "tp"),
        P("ep", None, "tp"),
        P("ep", "tp", None),
        P(),
    )
    out_specs = (P(("grp", "ep"), None), P(("grp", "ep"), "tp", None))
    return jax.shard_map(
        per_device, mesh=mesh, in_specs=in_specs, out_specs=out_specs, check_vma=False
    )
```

profile of v0, /device:TPU:40, one launch (start us, length us, event | category | flops | bytes accessed | tf_op | source)
XLA Modules:
  0.0 197.4 jit_solution(56538877208457532)
XLA Ops:
  7.2 0.0 copy-start
  7.2 0.8 exp.20
  8.0 1.9 convolution_convert_fusion.3
  9.9 0.0 copy-start.14
  9.9 0.0 copy-start.15
  9.9 0.0 copy-start.9
  9.9 0.1 copy.75
  10.1 0.3 fusion.60
  10.4 0.3 copy-done.14
  10.6 0.0 copy-done.15
  10.6 0.1 add_divide_fusion
  10.8 0.1 copy-done.9
  10.9 0.5 fusion.5
  11.4 1.4 fusion.6
  12.8 0.1 mul.223
  12.9 1.6 fusion.41
  14.4 0.4 fusion.36
  14.8 0.4 convolution_convert_fusion.2
  15.3 0.0 copy-start.13
  15.3 1.2 broadcast_in_dim.24
  16.4 4.6 %all-to-all-start = ((bf16[4,64,2048]{2,1,0:T(8,128)(2,1)}), bf16[4,64,2048]{2,1,0:T(8,128)(2,1)}, u32[]{:S(2)}, u32[]{:S(2)}) async-start(bf16[4,64,2048]{2,1,0:T(8,128)(2,1)} %broadcast_in_dim.24), calls=%async_computation | async-start | bytes 2097152 | tf_op jit(solution)/shard_map/all_to_all | solution.py:12
  21.0 0.1 convert_reduce_fusion.1
  21.1 0.1 reduce_window_sum.11
  21.2 0.2 select_reduce_fusion.2
  21.4 0.1 fusion.51
  21.5 14.8 %all-to-all-done = bf16[4,64,2048]{2,1,0:T(8,128)(2,1)} async-done(((bf16[4,64,2048]{2,1,0:T(8,128)(2,1)}), bf16[4,64,2048]{2,1,0:T(8,128)(2,1)}, u32[]{:S(2)}, u32[]{:S(2)}) %all-to-all-start) | async-done | bytes 1048608 | tf_op jit(solution)/shard_map/all_to_all | solution.py:12
  36.3 1.4 convert_reduce_fusion
  37.7 1.1 fusion.59
  38.8 1.2 multiply_reduce_fusion.1
  40.0 1.1 fusion.23
  41.1 0.0 copy-start.3
  41.2 0.7 copy-done.3
  41.8 1.5 convolution_convert_fusion.1
  43.3 2.3 %reshape.109 = bf16[32,2,4,2048]{3,2,1,0:T(4,128)(2,1)} reshape(bf16[256,2048]{1,0:T(8,128)(2,1)} %convolution_convert_fusion.1) | data formatting | bytes 2097152 | tf_op jit(solution)/shard_map/reshape | solution.py:170
  45.6 1.0 constant_dynamic-slice_fusion
  46.6 46.5 %all_to_all.25 = bf16[32,2,4,512]{3,2,1,0:T(4,128)(2,1)S(1)} all-to-all(bf16[32,2,4,512]{3,2,1,0:T(4,128)(2,1)S(1)} %constant_dynamic-slice_fusion), channel_id=1, replica_groups=mesh['grp'=2,'ep'=32,'tp'=4] {'ep'}, dimensions={0} | all-to-all | bytes 524288 | tf_op jit(solution)/shard_map/all_to_all | solution.py:176
  93.2 0.1 copy.76
  93.3 0.1 broadcast_in_dim.34
  93.4 0.0 copy-start.6
  93.4 18.0 %all_to_all.26 = bf16[4,32,2,4,512]{4,1,3,2,0:T(8,128)(2,1)S(1)} all-to-all(bf16[4,32,2,4,512]{4,1,3,2,0:T(8,128)(2,1)S(1)} %broadcast_in_dim.34), channel_id=1, replica_groups=mesh['grp'=2,'ep'=32,'tp'=4] {'tp'}, dimensions={0} | all-to-all | bytes 2097152 | tf_op jit(solution)/shard_map/all_to_all | solution.py:12
  111.4 0.1 copy.89
  111.6 1.0 copy-done.1
  112.6 1.2 fusion.7
  113.7 3.8 %convolution_convert_fusion = bf16[2,32,4,2048]{3,1,2,0:T(8,128)(2,1)} fusion(bf16[2,256,2048]{2,1,0:T(8,128)(2,1)S(1)} %copy-done, bf16[32,2,4,2048]{3,0,2,1:T(8,128)(2,1)} %bitcast.85, bf16[2,2048,256]{2,1,0:T(8,128)(2,1)} %param.33, f32[32,2,4,256]{3,0,2,1:T(8,128)} %fusion.7), kind=kOutput, calls=%fused_computation | convolution fusion | flops 537788416 | bytes 6553600 | tf_op jit(solution)/shard_map/njcf,jfd->njcd/dot_general | solution.py:182
  117.5 1.4 copy.95
  118.8 17.5 %all_to_all.27 = bf16[4,32,2,4,512]{4,1,3,2,0:T(8,128)(2,1)} all-to-all(bf16[4,32,2,4,512]{4,1,3,2,0:T(8,128)(2,1)S(1)} %bitcast.88), channel_id=1, replica_groups=mesh['grp'=2,'ep'=32,'tp'=4] {'tp'}, dimensions={0} | all-to-all | bytes 2097152 | tf_op jit(solution)/shard_map/all_to_all | solution.py:38
  136.3 2.2 %reduce_sum.130 = bf16[32,2,4,512]{3,0,2,1:T(8,128)(2,1)} reduce(bf16[4,32,2,4,512]{4,1,3,2,0:T(8,128)(2,1)} %all_to_all.27, bf16[]{:T(256)} %constant.58.clone.1), dimensions={0}, to_apply=%region_12.13 | reduce | flops 393216 | bytes 1310722 | tf_op jit(solution)/shard_map/reduce_sum | solution.py:39
  138.5 1.2 copy.80
  139.7 26.5 %all_to_all.28 = bf16[32,2,4,512]{3,2,1,0:T(4,128)(2,1)} all-to-all(bf16[32,2,4,512]{3,2,1,0:T(4,128)(2,1)S(1)} %copy.80), channel_id=1, replica_groups=mesh['grp'=2,'ep'=32,'tp'=4] {'ep'}, dimensions={0} | all-to-all | bytes 524288 | tf_op jit(solution)/shard_map/all_to_all | solution.py:188
  166.2 1.7 reshape.112
  167.9 0.1 all-gather.2.cloned.1.call-update
  168.0 0.0 copy-start.4
  168.0 0.0 copy-start.10
  168.0 1.5 pad_maximum_fusion
  169.5 0.0 copy-start.2
  169.5 1.3 copy.81
  170.9 0.2 fusion.63
  171.1 0.2 select_reduce_fusion.1
  171.3 0.2 fusion.61
  171.5 0.1 select_reduce_fusion
  171.7 16.1 %all-gather.2.cloned.1.call-done = bf16[256,2048]{1,0:T(8,128)(2,1)} async-done(((bf16[256,512]{1,0:T(8,128)(2,1)}), bf16[256,2048]{1,0:T(8,128)(2,1)}) %all-gather.2.cloned.1.call-update) | async-done | bytes 1048592 | tf_op jit(solution)/shard_map/all_gather | solution.py:192
  187.8 1.7 fusion.62
  189.4 0.2 multiply_reduce_fusion
  189.7 0.8 multiply_convert_fusion
  (32 shorter events, 0.1 us)
Async XLA Ops:
  7.2 106.6 %copy-start = (bf16[2,256,2048]{2,1,0:T(8,128)(2,1)S(1)}, bf16[2,256,2048]{2,1,0:T(8,128)(2,1)}, u32[]{:S(2)}) copy-start(bf16[2,256,2048]{2,1,0:T(8,128)(2,1)} %param.34) | copy-start | bytes 6291460
  7.2 2.9 %copy-start.5 = (f32[64,24,128]{2,1,0:T(8,128)S(1)}, f32[64,24,128]{2,1,0:T(8,128)}, u32[]{:S(2)}) copy-start(f32[64,24,128]{2,1,0:T(8,128)} %param.19) | copy-start | bytes 2359300
  9.9 0.7 copy-start.14
  9.9 0.7 copy-start.15
  9.9 0.9 copy-start.9
  10.9 1.9 copy-start.17
  10.9 2.0 %copy-start.8 = (f32[24,16,128]{2,1,0:T(8,128)S(1)}, f32[24,16,128]{2,1,0:T(8,128)}, u32[]{:S(2)}) copy-start(f32[24,16,128]{2,1,0:T(8,128)} %param.26) | copy-start | bytes 589828
  12.9 2.0 %copy-start.7 = (bf16[384,2048]{1,0:T(8,128)(2,1)S(1)}, bf16[384,2048]{1,0:T(8,128)(2,1)}, u32[]{:S(2)}) copy-start(bf16[384,2048]{1,0:T(8,128)(2,1)} %param.28) | copy-start | bytes 4718596
  15.3 5.8 %copy-start.13 = (s32[64,2]{0,1:T(2,128)S(1)}, s32[64,2]{0,1:T(2,128)}, u32[]{:S(2)}) copy-start(s32[64,2]{0,1:T(2,128)} %param.20) | copy-start | bytes 1540
  16.4 19.8 %all-to-all-start = ((bf16[4,64,2048]{2,1,0:T(8,128)(2,1)}), bf16[4,64,2048]{2,1,0:T(8,128)(2,1)}, u32[]{:S(2)}, u32[]{:S(2)}) async-start(bf16[4,64,2048]{2,1,0:T(8,128)(2,1)} %broadcast_in_dim.24), calls=%async_computation | async-start | bytes 2097152 | tf_op jit(solution)/shard_map/all_to_all | solution.py:12
  21.0 19.0 %copy-start.11 = (f32[2048]{0:T(1024)S(1)}, f32[2048]{0:T(1024)}, u32[]{:S(2)}) copy-start(f32[2048]{0:T(1024)} %param.29) | copy-start | bytes 24580
  21.0 166.7 %all-gather.2.cloned.1.call-start = ((), (), s32[]{:S(2)}) async-start(), calls=%async_computation.5 | async-start | bytes 1310720 | tf_op jit(solution)/shard_map/all_gather | solution.py:192
  41.1 0.7 copy-start.3
  93.4 19.2 %copy-start.6 = (bf16[2,2048,256]{2,1,0:T(8,128)(2,1)S(1)}, bf16[2,2048,256]{2,1,0:T(8,128)(2,1)}, u32[]{:S(2)}) copy-start(bf16[2,2048,256]{2,1,0:T(8,128)(2,1)} %param.32) | copy-start | bytes 6291460
  111.6 1.0 copy-start.1
  168.0 2.9 %copy-start.4 = (bf16[64,2048]{1,0:T(8,128)(2,1)S(1)}, bf16[64,2048]{1,0:T(8,128)(2,1)}, u32[]{:S(2)}) copy-start(bf16[64,2048]{1,0:T(8,128)(2,1)} %copy-done.3) | copy-start | bytes 786436
  168.0 2.9 %copy-start.10 = (bf16[2048,64]{0,1:T(8,128)(2,1)S(1)}, bf16[2048,64]{0,1:T(8,128)(2,1)}, u32[]{:S(2)}) copy-start(bf16[2048,64]{0,1:T(8,128)(2,1)} %param.31) | copy-start | bytes 786436
  168.0 3.3 %copy-start.12 = (bf16[2048,4]{0,1:T(4,128)(2,1)S(1)}, bf16[2048,4]{0,1:T(4,128)(2,1)}, u32[]{:S(2)}) copy-start(bf16[2048,4]{0,1:T(4,128)(2,1)} %param.30) | copy-start | bytes 49156
  169.5 18.3 %copy-start.2 = (bf16[64,2048]{1,0:T(8,128)(2,1)S(1)}, bf16[64,2048]{1,0:T(8,128)(2,1)}, u32[]{:S(2)}) copy-start(bf16[64,2048]{1,0:T(8,128)(2,1)} %param.18) | copy-start | bytes 786436
  170.8 18.8 %copy-start.16 = (f32[2048]{0:T(1024)S(1)}, f32[2048]{0:T(1024)}, u32[]{:S(2)}) copy-start(f32[2048]{0:T(1024)} %param.35) | copy-start | bytes 24580
Sparse Core Ops, SparseCore 0:
  168.1 19.5 all-gather.1
where the time goes:
time: 198 us; the launch traced here: 197 us
  blocking collectives  109 us (55%)
  waiting for transfers between devices  30.9 us (16%)
  matrix products  14.6 us (7%)
  between operations  14.4 us (7%)
  local copies, waits for them, and re-layouts  13.8 us (7%)
  other arithmetic  10.5 us (5%)
  starting transfers between devices  4.58 us (2%)
    all_to_all x1, blocking collectives, per_device(): lax.all_to_all(own_columns, 'ep', split_axis=0, concat_axis=0, tiled=True)  46.5 us
    all_to_all x1, blocking collectives, per_device(): lax.all_to_all(share, 'ep', split_axis=0, concat_axis=0, tiled=True)  26.5 us
    all_to_all x1, blocking collectives, sent_to_all(): lax.all_to_all(jnp.broadcast_to(x[None], (devices, *x.shape)), axis, 0, 0...  18 us
    all_to_all x1, blocking collectives, sent_and_summed(): parts = lax.all_to_all(split_up(x, dim, devices), axis, 0, 0, tiled=True)  17.5 us
    all_gather x1, waiting for transfers between devices, per_device(): lax.all_gather(flat_rows, 'tp', axis=1, tiled=True).astype(jnp.float32)  16.1 us
    all_to_all x1, waiting for transfers between devices, sent_to_all(): lax.all_to_all(jnp.broadcast_to(x[None], (devices, *x.shape)), axis, 0, 0...  14.8 us
    all_to_all x1, starting transfers between devices, sent_to_all(): lax.all_to_all(jnp.broadcast_to(x[None], (devices, *x.shape)), axis, 0, 0...  4.58 us
  transfers between devices with their start and end apart: 2, of which 2 were waited for; matrix products, arithmetic and copies ran while one was open for 2% of the time, Pallas kernels for 0%

commit v1 on v0

--- a/solution.py
+++ b/solution.py
@@ -1,3 +1,4 @@
+import functools
 import jax
 import jax.numpy as jnp
 from jax import lax
@@ -5,6 +6,17 @@
 
 residual_scale = 8.0**0.25
 norm_eps = 1e-05
+
+
+def _load_leaves(mat, which_dim):
+    z_new = lax.axis_size("tp")
+    q_next = jnp.stack(z_new * [mat], 0)
+    newest = lax.all_to_all(q_next, "tp", 0, 0)
+    wide_out = jnp.concatenate(newest, which_dim)
+    return wide_out
+
+
+rest_yards = functools.partial(_load_leaves, which_dim=1)
 
 
 def sent_to_all(x, axis):
@@ -187,11 +199,7 @@
     ).astype(jnp.bfloat16)
     returned_rows = lax.all_to_all(share, "ep", split_axis=0, concat_axis=0, tiled=True)
     flat_rows = returned_rows.reshape(total_slots, returned_rows.shape[3])
-    moe = jnp.dot(
-        combine_map,
-        lax.all_gather(flat_rows, "tp", axis=1, tiled=True).astype(jnp.float32),
-        precision=top_precision,
-    )
+    moe = jnp.dot(combine_map, rest_yards(flat_rows).astype(jnp.float32), precision=top_precision)
     layer_out = normalize(residual_scale * hidden_state + moe, gain_moe).astype(jnp.bfloat16)
     return (layer_out, new_state)
 

time: 198 us -> 188 us (0.949)
  blocking collectives: 109 us -> 82.1 us
  waiting for transfers between devices: 30.9 us -> 47.7 us
  between operations: 14.4 us -> 0.98 us
  starting transfers between devices: 4.58 us -> 14.3 us
  local copies, waits for them, and re-layouts: 13.8 us -> 16.7 us
    all_to_all x0 -> x2, waiting for transfers between devices: none -> 32.9 us  [the longest x1 18.8 us: per_device(): lax.all_to_all(share, 'ep', split_axis=0, concat_axis=0, tiled=True)]
    all_to_all x1 -> x0, blocking collectives: 26.5 us -> none  [per_device(): lax.all_to_all(share, 'ep', split_axis=0, concat_axis=0, tiled=True)]
    all_gather x1 -> x0, waiting for transfers between devices: 16.1 us -> none  [per_device(): lax.all_gather(flat_rows, 'tp', axis=1, tiled=True).astype(jnp.float32)]
    all_to_all x0 -> x2, starting transfers between devices: none -> 9.72 us  [the longest x1 5.4 us: per_device(): lax.all_to_all(share, 'ep', split_axis=0, concat_axis=0, tiled=True)]
    another operation x0 -> x3, local copies, waits for them, and re-layouts: none -> 3.95 us  [_load_leaves(): q_next = jnp.stack(z_new * [mat], 0)]
  transfers between devices with their start and end apart: 2 -> 3, of which waited for: 2 -> 3; matrix products, arithmetic and copies ran while one was open for 2% -> 2% of each run, Pallas kernels for 0% -> 0%
where the time goes in v1:
time: 188 us; the launch traced here: 187 us
  blocking collectives  82.1 us (44%)
  waiting for transfers between devices  47.7 us (25%)
  local copies, waits for them, and re-layouts  16.7 us (9%)
  matrix products  14.7 us (8%)
  starting transfers between devices  14.3 us (8%)
  other arithmetic  10.5 us (6%)
    all_to_all x1, blocking collectives, per_device(): lax.all_to_all(own_columns, 'ep', split_axis=0, concat_axis=0, tiled=True)  46.5 us
    all_to_all x1, waiting for transfers between devices, per_device(): lax.all_to_all(share, 'ep', split_axis=0, concat_axis=0, tiled=True)  18.8 us
    all_to_all x1, blocking collectives, sent_to_all(): lax.all_to_all(jnp.broadcast_to(x[None], (devices, *x.shape)), axis, 0, 0...  18 us
    all_to_all x1, blocking collectives, sent_and_summed(): parts = lax.all_to_all(split_up(x, dim, devices), axis, 0, 0, tiled=True)  17.5 us
    all_to_all x1, waiting for transfers between devices, sent_to_all(): lax.all_to_all(jnp.broadcast_to(x[None], (devices, *x.shape)), axis, 0, 0...  14.8 us
    all_to_all x1, waiting for transfers between devices, _load_leaves(): newest = lax.all_to_all(q_next, 'tp', 0, 0)  14.1 us
    all_to_all x1, starting transfers between devices, per_device(): lax.all_to_all(share, 'ep', split_axis=0, concat_axis=0, tiled=True)  5.4 us
    all_to_all x1, starting transfers between devices, sent_to_all(): lax.all_to_all(jnp.broadcast_to(x[None], (devices, *x.shape)), axis, 0, 0...  4.58 us
  transfers between devices with their start and end apart: 3, of which 3 were waited for; matrix products, arithmetic and copies ran while one was open for 2% of the time, Pallas kernels for 0%

profile of v1, /device:TPU:40, one launch (start us, length us, event | category | flops | bytes accessed | tf_op | source)
XLA Modules:
  0.0 186.9 jit_solution(1396444726638524079)
XLA Ops:
  0.6 0.0 copy-start
  0.7 0.8 exp.20
  1.5 1.9 %convolution_convert_fusion.3 = bf16[64,384]{1,0:T(8,128)(2,1)S(1)} fusion(bf16[64,2048]{1,0:T(8,128)(2,1)} %param.18, bf16[2048,384]{1,0:T(8,128)(2,1)} %param.21), kind=kOutput, calls=%fused_computation.21 | convolution fusion | flops 100687872 | bytes 1884160 | tf_op jit(solution)/shard_map/dot_general | solution.py:152
  3.4 0.0 copy-start.15
  3.4 0.0 copy-start.16
  3.4 0.0 copy-start.10
  3.4 0.1 copy.75
  3.5 0.3 fusion.60
  3.8 0.3 copy-done.15
  4.1 0.0 copy-done.16
  4.1 0.1 add_divide_fusion
  4.2 0.1 copy-done.10
  4.3 0.5 fusion.5
  4.8 1.4 fusion.6
  6.2 0.1 mul.223
  6.3 1.6 fusion.41
  7.9 0.4 fusion.36
  8.3 0.4 convolution_convert_fusion.2
  8.7 1.2 broadcast_in_dim.24
  9.9 4.6 %all-to-all-start = ((bf16[4,64,2048]{2,1,0:T(8,128)(2,1)}), bf16[4,64,2048]{2,1,0:T(8,128)(2,1)}, u32[]{:S(2)}, u32[]{:S(2)}) async-start(bf16[4,64,2048]{2,1,0:T(8,128)(2,1)} %broadcast_in_dim.24), calls=%async_computation | async-start | bytes 2097152 | tf_op jit(solution)/shard_map/all_to_all | solution.py:24
  14.5 0.1 convert_reduce_fusion.1
  14.6 0.1 reduce_window_sum.11
  14.7 0.2 select_reduce_fusion.2
  14.8 0.1 fusion.51
  14.9 14.8 %all-to-all-done = bf16[4,64,2048]{2,1,0:T(8,128)(2,1)} async-done(((bf16[4,64,2048]{2,1,0:T(8,128)(2,1)}), bf16[4,64,2048]{2,1,0:T(8,128)(2,1)}, u32[]{:S(2)}, u32[]{:S(2)}) %all-to-all-start) | async-done | bytes 1048608 | tf_op jit(solution)/shard_map/all_to_all | solution.py:24
  29.7 1.4 convert_reduce_fusion
  31.2 1.1 fusion.59
  32.3 1.2 multiply_reduce_fusion.1
  33.5 1.1 fusion.23
  34.6 0.0 copy-start.3
  34.6 0.7 copy-done.3
  35.3 1.5 convolution_convert_fusion.1
  36.8 2.3 %reshape.114 = bf16[32,2,4,2048]{3,2,1,0:T(4,128)(2,1)} reshape(bf16[256,2048]{1,0:T(8,128)(2,1)} %convolution_convert_fusion.1) | data formatting | bytes 2097152 | tf_op jit(solution)/shard_map/reshape | solution.py:182
  39.0 1.0 constant_dynamic-slice_fusion
  40.1 46.5 %all_to_all.30 = bf16[32,2,4,512]{3,2,1,0:T(4,128)(2,1)S(1)} all-to-all(bf16[32,2,4,512]{3,2,1,0:T(4,128)(2,1)S(1)} %constant_dynamic-slice_fusion), channel_id=1, replica_groups=mesh['grp'=2,'ep'=32,'tp'=4] {'ep'}, dimensions={0} | all-to-all | bytes 524288 | tf_op jit(solution)/shard_map/all_to_all | solution.py:188
  86.6 0.1 copy.76
  86.7 0.1 broadcast_in_dim.34
  86.8 0.0 copy-start.7
  86.8 18.0 %all_to_all.31 = bf16[4,32,2,4,512]{4,1,3,2,0:T(8,128)(2,1)S(1)} all-to-all(bf16[4,32,2,4,512]{4,1,3,2,0:T(8,128)(2,1)S(1)} %broadcast_in_dim.34), channel_id=1, replica_groups=mesh['grp'=2,'ep'=32,'tp'=4] {'tp'}, dimensions={0} | all-to-all | bytes 2097152 | tf_op jit(solution)/shard_map/all_to_all | solution.py:24
  104.9 0.1 copy.90
  105.0 1.0 copy-done.1
  106.0 1.2 fusion.7
  107.2 3.8 %convolution_convert_fusion = bf16[2,32,4,2048]{3,1,2,0:T(8,128)(2,1)} fusion(bf16[2,256,2048]{2,1,0:T(8,128)(2,1)S(1)} %copy-done, bf16[32,2,4,2048]{3,0,2,1:T(8,128)(2,1)} %bitcast.88, bf16[2,2048,256]{2,1,0:T(8,128)(2,1)} %param.33, f32[32,2,4,256]{3,0,2,1:T(8,128)} %fusion.7), kind=kOutput, calls=%fused_computation | convolution fusion | flops 537788416 | bytes 6553600 | tf_op jit(solution)/shard_map/njcf,jfd->njcd/dot_general | solution.py:194
  110.9 1.4 copy.96
  112.3 17.5 %all_to_all.32 = bf16[4,32,2,4,512]{4,1,3,2,0:T(8,128)(2,1)} all-to-all(bf16[4,32,2,4,512]{4,1,3,2,0:T(8,128)(2,1)S(1)} %bitcast.91), channel_id=1, replica_groups=mesh['grp'=2,'ep'=32,'tp'=4] {'tp'}, dimensions={0} | all-to-all | bytes 2097152 | tf_op jit(solution)/shard_map/all_to_all | solution.py:50
  129.8 2.2 %reduce_sum.130 = bf16[32,2,4,512]{3,0,2,1:T(8,128)(2,1)} reduce(bf16[4,32,2,4,512]{4,1,3,2,0:T(8,128)(2,1)} %all_to_all.32, bf16[]{:T(256)} %constant.58.clone.1), dimensions={0}, to_apply=%region_12.13 | reduce | flops 393216 | bytes 1310722 | tf_op jit(solution)/shard_map/reduce_sum | solution.py:51
  132.0 1.9 copy.80
  133.8 5.4 %all-to-all-start.4 = ((bf16[32,2,4,512]{3,2,1,0:T(4,128)(2,1)}), bf16[32,2,4,512]{3,2,1,0:T(4,128)(2,1)}, u32[]{:S(2)}, u32[]{:S(2)}) async-start(bf16[32,2,4,512]{3,2,1,0:T(4,128)(2,1)} %copy.80), calls=%async_computation.4 | async-start | bytes 524288 | tf_op jit(solution)/shard_map/all_to_all | solution.py:200
  139.2 0.0 copy-start.4
  139.2 1.5 pad_maximum_fusion
  140.7 1.3 copy.82
  142.1 0.2 fusion.63
  142.3 0.2 select_reduce_fusion.1
  142.5 18.8 %all-to-all-done.4 = bf16[32,2,4,512]{3,2,1,0:T(4,128)(2,1)} async-done(((bf16[32,2,4,512]{3,2,1,0:T(4,128)(2,1)}), bf16[32,2,4,512]{3,2,1,0:T(4,128)(2,1)}, u32[]{:S(2)}, u32[]{:S(2)}) %all-to-all-start.4) | async-done | bytes 262176 | tf_op jit(solution)/shard_map/all_to_all | solution.py:200
  161.3 1.7 stack_reshape.2
  163.0 1.1 copy.81
  164.1 1.1 stack.3
  165.2 4.3 %all-to-all-start.5 = ((bf16[4,256,512]{1,2,0:T(8,128)(2,1)}), bf16[4,256,512]{1,2,0:T(8,128)(2,1)}, u32[]{:S(2)}, u32[]{:S(2)}) async-start(bf16[4,256,512]{1,2,0:T(8,128)(2,1)} %stack.3), calls=%async_computation.5 | async-start | bytes 2097152 | tf_op jit(solution)/shard_map/all_to_all | solution.py:14
  169.6 0.2 fusion.61
  169.8 0.1 select_reduce_fusion
  170.0 14.1 %all-to-all-done.5 = bf16[4,256,512]{1,2,0:T(8,128)(2,1)} async-done(((bf16[4,256,512]{1,2,0:T(8,128)(2,1)}), bf16[4,256,512]{1,2,0:T(8,128)(2,1)}, u32[]{:S(2)}, u32[]{:S(2)}) %all-to-all-start.5) | async-done | bytes 1048608 | tf_op jit(solution)/shard_map/all_to_all | solution.py:14
  184.1 1.8 fusion.62
  185.9 0.2 multiply_reduce_fusion
  186.1 0.8 multiply_convert_fusion
  (36 shorter events, 0.2 us)
Async XLA Ops:
  0.6 106.6 %copy-start = (bf16[2,256,2048]{2,1,0:T(8,128)(2,1)S(1)}, bf16[2,256,2048]{2,1,0:T(8,128)(2,1)}, u32[]{:S(2)}) copy-start(bf16[2,256,2048]{2,1,0:T(8,128)(2,1)} %param.34) | copy-start | bytes 6291460
  0.6 2.9 %copy-start.6 = (f32[64,24,128]{2,1,0:T(8,128)S(1)}, f32[64,24,128]{2,1,0:T(8,128)}, u32[]{:S(2)}) copy-start(f32[64,24,128]{2,1,0:T(8,128)} %param.19) | copy-start | bytes 2359300
  3.4 0.7 copy-start.15
  3.4 0.7 copy-start.16
  3.4 0.9 copy-start.10
  4.3 1.9 %copy-start.18 = (f32[384]{0:T(512)S(1)}, f32[384]{0:T(512)}, u32[]{:S(2)}) copy-start(f32[384]{0:T(512)} %param.27) | copy-start | bytes 4612
  4.3 2.0 %copy-start.9 = (f32[24,16,128]{2,1,0:T(8,128)S(1)}, f32[24,16,128]{2,1,0:T(8,128)}, u32[]{:S(2)}) copy-start(f32[24,16,128]{2,1,0:T(8,128)} %param.26) | copy-start | bytes 589828
  6.3 2.0 %copy-start.8 = (bf16[384,2048]{1,0:T(8,128)(2,1)S(1)}, bf16[384,2048]{1,0:T(8,128)(2,1)}, u32[]{:S(2)}) copy-start(bf16[384,2048]{1,0:T(8,128)(2,1)} %param.28) | copy-start | bytes 4718596
  8.7 5.8 %copy-start.14 = (s32[64,2]{0,1:T(2,128)S(1)}, s32[64,2]{0,1:T(2,128)}, u32[]{:S(2)}) copy-start(s32[64,2]{0,1:T(2,128)} %param.20) | copy-start | bytes 1540
  9.9 19.8 %all-to-all-start = ((bf16[4,64,2048]{2,1,0:T(8,128)(2,1)}), bf16[4,64,2048]{2,1,0:T(8,128)(2,1)}, u32[]{:S(2)}, u32[]{:S(2)}) async-start(bf16[4,64,2048]{2,1,0:T(8,128)(2,1)} %broadcast_in_dim.24), calls=%async_computation | async-start | bytes 2097152 | tf_op jit(solution)/shard_map/all_to_all | solution.py:24
  14.5 19.0 %copy-start.12 = (f32[2048]{0:T(1024)S(1)}, f32[2048]{0:T(1024)}, u32[]{:S(2)}) copy-start(f32[2048]{0:T(1024)} %param.29) | copy-start | bytes 24580
  34.6 0.7 copy-start.3
  86.8 19.2 %copy-start.7 = (bf16[2,2048,256]{2,1,0:T(8,128)(2,1)S(1)}, bf16[2,2048,256]{2,1,0:T(8,128)(2,1)}, u32[]{:S(2)}) copy-start(bf16[2,2048,256]{2,1,0:T(8,128)(2,1)} %param.32) | copy-start | bytes 6291460
  105.0 1.0 copy-start.1
  133.8 27.4 %all-to-all-start.4 = ((bf16[32,2,4,512]{3,2,1,0:T(4,128)(2,1)}), bf16[32,2,4,512]{3,2,1,0:T(4,128)(2,1)}, u32[]{:S(2)}, u32[]{:S(2)}) async-start(bf16[32,2,4,512]{3,2,1,0:T(4,128)(2,1)} %copy.80), calls=%async_computation.4 | async-start | bytes 524288 | tf_op jit(solution)/shard_map/all_to_all | solution.py:200
  139.2 2.8 %copy-start.4 = (bf16[64,2048]{1,0:T(8,128)(2,1)S(1)}, bf16[64,2048]{1,0:T(8,128)(2,1)}, u32[]{:S(2)}) copy-start(bf16[64,2048]{1,0:T(8,128)(2,1)} %copy-done.3) | copy-start | bytes 786436
  139.2 2.8 %copy-start.11 = (bf16[2048,64]{0,1:T(8,128)(2,1)S(1)}, bf16[2048,64]{0,1:T(8,128)(2,1)}, u32[]{:S(2)}) copy-start(bf16[2048,64]{0,1:T(8,128)(2,1)} %param.31) | copy-start | bytes 786436
  163.0 6.6 %copy-start.5 = (bf16[64,2048]{1,0:T(8,128)(2,1)S(1)}, bf16[64,2048]{1,0:T(8,128)(2,1)}, u32[]{:S(2)}) copy-start(bf16[64,2048]{1,0:T(8,128)(2,1)} %copy-done.3) | copy-start | bytes 786436
  163.0 6.6 %copy-start.13 = (bf16[2048,4]{0,1:T(4,128)(2,1)S(1)}, bf16[2048,4]{0,1:T(4,128)(2,1)}, u32[]{:S(2)}) copy-start(bf16[2048,4]{0,1:T(4,128)(2,1)} %param.30) | copy-start | bytes 49156
  163.0 21.1 %copy-start.2 = (bf16[64,2048]{1,0:T(8,128)(2,1)S(1)}, bf16[64,2048]{1,0:T(8,128)(2,1)}, u32[]{:S(2)}) copy-start(bf16[64,2048]{1,0:T(8,128)(2,1)} %param.18) | copy-start | bytes 786436
  165.2 18.8 %all-to-all-start.5 = ((bf16[4,256,512]{1,2,0:T(8,128)(2,1)}), bf16[4,256,512]{1,2,0:T(8,128)(2,1)}, u32[]{:S(2)}, u32[]{:S(2)}) async-start(bf16[4,256,512]{1,2,0:T(8,128)(2,1)} %stack.3), calls=%async_computation.5 | async-start | bytes 2097152 | tf_op jit(solution)/shard_map/all_to_all | solution.py:14
  169.6 16.5 %copy-start.17 = (f32[2048]{0:T(1024)S(1)}, f32[2048]{0:T(1024)}, u32[]{:S(2)}) copy-start(f32[2048]{0:T(1024)} %param.35) | copy-start | bytes 24580
